TPU v7x, 32 devices: a whole 2x2x4 slice. The times are simulated.
32 devices in a mesh: grp: 2 (over y), ep: 8 (over z, x), tp: 2 (over core).
Axes of the slice: x: 2, y: 2, z: 4, core: 2. Of those that a mesh axis runs over, the one named last changes fastest.
Arguments:
- hidden_state: bfloat16 [1024, 1024], P(('grp', 'ep'), 'tp'), parts along dimension 0, may hold values from -6 to 6
- expert_ids: int32 [1024, 4], P(('grp', 'ep')), parts along dimension 0, may hold values from 0 to 7, all different within a row; in each aligned block of 64 rows (0 to 63, 64 to 127, ...) at most 64 rows name the same one
- route_weight: float32 [1024, 4], P(('grp', 'ep')), parts along dimension 0, may hold values from 0.1 to 1
- gate_matrix: bfloat16 [8, 1024, 2048], P('ep', None, 'tp'), may hold values from -0.1875 to 0.1875
- up_matrix: bfloat16 [8, 1024, 2048], P('ep', None, 'tp'), may hold values from -0.1875 to 0.1875
- down_matrix: bfloat16 [8, 2048, 1024], P('ep', 'tp'), may hold values from -2 to 2
- norm_gain: float32 [1024], P('tp'), may hold values from 0.1 to 1.9
Outputs:
- normed_out: bfloat16 [1024, 1024], P(('grp', 'ep'), 'tp'), parts along dimension 0
There are 2 independent parts, one for each index of `grp`. A program takes and returns all parts, laid end to end along the dimension named above; an argument that names none is the same for every part. Nothing has to cross between parts.
Inputs may be any that keep to these rules, and one draw needn't show every extreme that they name: `expert_ids`: each row names 4 different experts. Within the rows of one index of ep (aligned blocks of 64 rows) no expert is named by more than 64 rows, and in some blocks one expert is named by exactly 64 rows. Every expert is named by some row.
All inputs are finite; a program needn't handle non-finite values.
Results may differ from a plain program's by a relative error of at most 0.0065.
Values may be sent and summed in bfloat16 or wider, within the bound.
A program may use at most 64 MiB of HBM per device.

v0:
```python
import jax
import jax.numpy as jnp
from jax import lax
from jax.sharding import PartitionSpec as P

D = 1024
norm_eps = 1e-05


def slot_numbers(block_ids, expert_count):
    onehot = (block_ids[..., None] == jnp.arange(expert_count, dtype=jnp.int32)).astype(jnp.int32)
    earlier = jnp.cumsum(onehot, axis=-2) - onehot
    return jnp.sum(earlier * onehot, axis=-1)


def expert_rows(buffer, gate_matrix, up_matrix, down_matrix):
    sources, item_count, feature_count = buffer.shape
    token_rows = buffer.reshape(sources * item_count, feature_count)
    gate_pre = jnp.dot(token_rows, gate_matrix[0], preferred_element_type=jnp.float32)
    up_pre = jnp.dot(token_rows, up_matrix[0], preferred_element_type=jnp.float32)
    activated = (jax.nn.silu(gate_pre) * up_pre).astype(jnp.bfloat16)
    partial_value = jnp.dot(activated, down_matrix[0], preferred_element_type=jnp.float32)
    summed = lax.psum_scatter(
        partial_value.reshape(sources, item_count, feature_count).astype(jnp.bfloat16),
        "tp",
        scatter_dimension=2,
        tiled=True,
    )
    return summed


def shards(hidden_state, expert_ids, route_weight, gate_matrix, up_matrix, down_matrix, norm_gain):
    tok_count, top_count = expert_ids.shape
    expert_count = lax.axis_size("ep")
    capacity = max(2, 2 * tok_count * top_count // expert_count)
    slot_total = expert_count * capacity
    slot_rank = slot_numbers(expert_ids.reshape(1, tok_count * top_count), expert_count)
    slot_index = expert_ids * capacity + slot_rank.reshape(tok_count, top_count)
    positions = jnp.arange(slot_total, dtype=jnp.int32)
    matches = slot_index[:, :, None] == positions[None, None, :]
    placing = jnp.transpose(jnp.any(matches, axis=1)).astype(jnp.bfloat16)
    combine = jnp.sum(jnp.where(matches, route_weight[:, :, None], 0.0), axis=1)
    outgoing = jnp.dot(placing, hidden_state, preferred_element_type=jnp.float32).astype(
        jnp.bfloat16
    )
    answers = expert_rows(
        lax.all_gather(
            lax.all_to_all(
                outgoing.reshape(expert_count, capacity, hidden_state.shape[1]),
                "ep",
                split_axis=0,
                concat_axis=0,
                tiled=True,
            ),
            "tp",
            axis=2,
            tiled=True,
        ),
        gate_matrix,
        up_matrix,
        down_matrix,
    )
    returned = lax.all_to_all(answers, "ep", split_axis=0, concat_axis=0, tiled=True)
    combined = jnp.dot(
        combine,
        returned.reshape(slot_total, returned.shape[2]).astype(jnp.float32),
        precision=lax.Precision.HIGHEST,
    )
    local_squares = jnp.sum(combined * combined, axis=1)
    total_squares = lax.psum(local_squares, "tp")
    inverse_rms = lax.rsqrt(total_squares / D + norm_eps)
    return (combined * inverse_rms[:, None] * norm_gain).astype(jnp.bfloat16)


def solution(mesh):
    placed = (
        P(("grp", "ep"), "tp"),
        P(("grp", "ep"), None),
        P(("grp", "ep"), None),
        P("ep", None, "tp"),
        P("ep", None, "tp"),
        P("ep", "tp", None),
        P("tp"),
    )
    return jax.shard_map(
        shards, mesh=mesh, in_specs=placed, out_specs=P(("grp", "ep"), "tp"), check_vma=False
    )
```

profile of v0, /device:TPU:0, one launch (start us, length us, event | category | flops | bytes accessed | tf_op | source)
XLA Modules:
  0.0 88.2 jit_solution(9417557024511087397)
XLA Ops:
  6.5 0.0 copy-start
  6.5 0.0 all-gather.2.cloned.1.call-start
  6.5 0.9 %copy.18 = s32[64,4]{1,0:T(8,128)S(1)} copy(s32[64,4]{0,1:T(4,128)} %param.8) | data formatting | bytes 2048 | tf_op args[1]
  7.5 0.1 eq.40
  7.6 0.6 reduce-window.6
  8.2 0.2 slice_reduce_fusion
  8.4 0.1 fusion.13
  8.5 0.1 reshape.139
  8.6 0.1 copy.19
  8.7 0.7 multiply_add_fusion
  9.4 0.1 fusion.11
  9.5 1.2 %convolution_convert_fusion = bf16[512,512]{1,0:T(8,128)(2,1)S(1)} fusion(pred[64,512]{1,0:T(8,128)(4,1)S(1)} %fusion.11, bf16[64,512]{1,0:T(8,128)(2,1)} %param.7), kind=kOutput, calls=%fused_computation.8 | convolution fusion | flops 33816576 | bytes 622592 | tf_op jit(solution)/shard_map/dot_general | solution.py:43
  10.7 21.7 %all_to_all.10 = bf16[8,64,512]{2,1,0:T(8,128)(2,1)} all-to-all(bf16[8,64,512]{2,1,0:T(8,128)(2,1)S(1)} %bitcast.41), channel_id=1, replica_groups=mesh['grp'=2,'ep'=8,'tp'=2] {'ep'}, dimensions={0} | all-to-all | bytes 1048576 | tf_op jit(solution)/shard_map/all_to_all | solution.py:48
  32.5 0.0 all-gather.2.cloned.1.call-update
  32.5 0.0 reduce-scatter.2.cloned.1.call-start
  32.5 8.2 %all-gather.2.cloned.1.call-done = bf16[8,64,1024]{2,1,0:T(8,128)(2,1)} async-done(((bf16[8,64,512]{2,1,0:T(8,128)(2,1)}), bf16[8,64,1024]{2,1,0:T(8,128)(2,1)}) %all-gather.2.cloned.1.call-update) | async-done | bytes 1048592 | tf_op jit(solution)/shard_map/all_gather | solution.py:47
  40.7 0.0 copy-done
  40.7 0.0 copy-start.3
  40.7 0.0 copy-start.5
  40.7 2.6 %fusion.4 = f32[512,1024]{1,0:T(8,128)S(1)} fusion(bf16[512,1024]{1,0:T(8,128)(2,1)} %bitcast.43, bf16[1,1024,1024]{2,1,0:T(8,128)(2,1)S(1)} %copy-done), kind=kOutput, calls=%fused_computation.4 | convolution fusion | flops 1073741824 | bytes 5242880 | tf_op jit(solution)/shard_map/dot_general | solution.py:19
  43.3 0.0 copy-done.3
  43.3 0.0 copy-done.5
  43.3 0.0 copy-start.4
  43.4 1.4 %multiply_convert_fusion = bf16[512,1024]{1,0:T(8,128)(2,1)S(1)} fusion(f32[512,1024]{1,0:T(8,128)S(1)} %fusion.4, bf16[512,1024]{1,0:T(8,128)(2,1)S(1)} %bitcast.44, bf16[1,1024,1024]{2,1,0:T(8,128)(2,1)S(1)} %copy-done.3), kind=kOutput, calls=%fused_computation.6 | convolution fusion | flops 1076887552 | bytes 6291456 | tf_op jit(solution)/shard_map/dot_general | solution.py:20
  44.7 0.2 copy-done.4
  44.9 2.2 %fusion.8 = bf16[8,64,1024]{2,1,0:T(8,128)(2,1)} fusion(bf16[8,64,1024]{2,1,0:T(8,128)(2,1)S(1)} %bitcast.45, bf16[1,1024,1024]{2,1,0:T(8,128)(2,1)S(1)} %copy-done.4), kind=kOutput, calls=%fused_computation.7 | convolution fusion | flops 1074266112 | bytes 4194304 | tf_op jit(solution)/shard_map/dot_general | solution.py:22
  47.2 0.0 copy-start.1
  47.2 0.0 copy-start.2
  47.2 0.0 reduce-scatter.2.cloned.1.call-update
  47.2 9.7 %reduce-scatter.2.cloned.1.call-done = bf16[8,64,512]{2,1,0:T(8,128)(2,1)} async-done(((bf16[8,64,1024]{2,1,0:T(8,128)(2,1)}), bf16[8,64,512]{2,1,0:T(8,128)(2,1)}) %reduce-scatter.2.cloned.1.call-update) | async-done | bytes 524304 | tf_op jit(solution)/shard_map/reduce_scatter | solution.py:23
  56.9 5.8 %all-to-all-start.1 = ((bf16[8,64,512]{2,1,0:T(8,128)(2,1)}), bf16[8,64,512]{2,1,0:T(8,128)(2,1)S(1)}, u32[]{:S(2)}, u32[]{:S(2)}) async-start(bf16[8,64,512]{2,1,0:T(8,128)(2,1)} %reduce-scatter.2.cloned.1.call-done), calls=%async_computation.2 | async-start | bytes 1048576 | tf_op jit(solution)/shard_map/all_to_all | solution.py:63
  62.7 0.0 copy-done.1
  62.7 0.1 select_reduce_fusion
  62.8 14.8 %all-to-all-done.1 = bf16[8,64,512]{2,1,0:T(8,128)(2,1)S(1)} async-done(((bf16[8,64,512]{2,1,0:T(8,128)(2,1)}), bf16[8,64,512]{2,1,0:T(8,128)(2,1)S(1)}, u32[]{:S(2)}, u32[]{:S(2)}) %all-to-all-start.1) | async-done | bytes 524320 | tf_op jit(solution)/shard_map/all_to_all | solution.py:63
  77.6 0.5 multiply_reduce_fusion
  78.1 2.5 %psum.7 = f32[64]{0:T(128)S(1)} all-reduce(f32[64]{0:T(128)S(1)} %get-tuple-element.5), channel_id=1, replica_groups=mesh['grp'=2,'ep'=8,'tp'=2] {'tp'}, use_global_device_ids=true, to_apply=%region_7.8 | all-reduce | flops 64 | bytes 512 | tf_op jit(solution)/shard_map/psum | solution.py:70
  80.6 0.0 copy-done.2
  80.6 0.7 multiply_convert_fusion.1
  (4 shorter events, 0.1 us)
Async XLA Ops:
  6.5 34.2 %copy-start = (bf16[1,1024,1024]{2,1,0:T(8,128)(2,1)S(1)}, bf16[1,1024,1024]{2,1,0:T(8,128)(2,1)}, u32[]{:S(2)}) copy-start(bf16[1,1024,1024]{2,1,0:T(8,128)(2,1)} %param.10) | copy-start | bytes 6291460
  6.5 34.2 %all-gather.2.cloned.1.call-start = ((), (), s32[]{:S(2)}) async-start(), calls=%async_computation.3 | async-start | bytes 1572864 | tf_op jit(solution)/shard_map/all_gather | solution.py:47
  32.5 24.4 %reduce-scatter.2.cloned.1.call-start = ((), (), s32[]{:S(2)}) async-start(), calls=%async_computation.4 | async-start | bytes 1572864 | tf_op jit(solution)/shard_map/reduce_scatter | solution.py:23
  40.7 2.6 %copy-start.3 = (bf16[1,1024,1024]{2,1,0:T(8,128)(2,1)S(1)}, bf16[1,1024,1024]{2,1,0:T(8,128)(2,1)}, u32[]{:S(2)}) copy-start(bf16[1,1024,1024]{2,1,0:T(8,128)(2,1)} %param.11) | copy-start | bytes 6291460
  40.7 2.6 %copy-start.5 = (bf16[8,64,1024]{2,1,0:T(8,128)(2,1)S(1)}, bf16[8,64,1024]{2,1,0:T(8,128)(2,1)}, u32[]{:S(2)}) copy-start(bf16[8,64,1024]{2,1,0:T(8,128)(2,1)} %all-gather.2.cloned.1.call-done) | copy-start | bytes 3145732
  43.3 1.6 %copy-start.4 = (bf16[1,1024,1024]{2,1,0:T(8,128)(2,1)S(1)}, bf16[1,1024,1024]{2,1,0:T(8,128)(2,1)}, u32[]{:S(2)}) copy-start(bf16[1,1024,1024]{2,1,0:T(8,128)(2,1)} %param.12) | copy-start | bytes 6291460
  47.2 15.5 %copy-start.1 = (f32[64,4]{0,1:T(4,128)S(1)}, f32[64,4]{0,1:T(4,128)}, u32[]{:S(2)}) copy-start(f32[64,4]{0,1:T(4,128)} %param.9) | copy-start | bytes 3076
  47.2 33.4 %copy-start.2 = (f32[512]{0:T(512)S(1)}, f32[512]{0:T(512)}, u32[]{:S(2)}) copy-start(f32[512]{0:T(512)} %param.13) | copy-start | bytes 6148
  56.9 20.7 %all-to-all-start.1 = ((bf16[8,64,512]{2,1,0:T(8,128)(2,1)}), bf16[8,64,512]{2,1,0:T(8,128)(2,1)S(1)}, u32[]{:S(2)}, u32[]{:S(2)}) async-start(bf16[8,64,512]{2,1,0:T(8,128)(2,1)} %reduce-scatter.2.cloned.1.call-done), calls=%async_computation.2 | async-start | bytes 1048576 | tf_op jit(solution)/shard_map/all_to_all | solution.py:63
Sparse Core Ops, SparseCore 0:
  32.6 8.0 all-gather.1
  47.3 9.5 reduce-scatter.1
where the time goes:
time: 88.5 us; the launch traced here: 88.2 us
  waiting for transfers between devices  32.7 us (37%)
  blocking collectives  24.2 us (27%)
  between operations  13.5 us (15%)
  matrix products  7.91 us (9%)
  starting transfers between devices  5.82 us (7%)
  other arithmetic  2.42 us (3%)
  local copies, waits for them, and re-layouts  1.65 us (2%)
    all_to_all x1, blocking collectives, shards(): lax.all_to_all(outgoing.reshape(expert_count, capacity, hidden_state.shap...  21.7 us
    all_to_all x1, waiting for transfers between devices, shards(): lax.all_to_all(answers, 'ep', split_axis=0, concat_axis=0, tiled=True)  14.8 us
    reduce_scatter x1, waiting for transfers between devices, expert_rows(): lax.psum_scatter(partial_value.reshape(sources, item_count, feature_count...  9.7 us
    all_gather x1, waiting for transfers between devices, shards(): lax.all_gather(lax.all_to_all(outgoing.reshape(expert_count, capacity, hi...  8.17 us
    all_to_all x1, starting transfers between devices, shards(): lax.all_to_all(answers, 'ep', split_axis=0, concat_axis=0, tiled=True)  5.78 us
    dot_general x1, matrix products, expert_rows(): jnp.dot(token_rows, gate_matrix[0], preferred_element_type=jnp.float32)  2.62 us
    psum x1, blocking collectives, shards(): total_squares = lax.psum(local_squares, 'tp')  2.47 us
    dot_general x1, matrix products, expert_rows(): jnp.dot(activated, down_matrix[0], preferred_element_type=jnp.float32)  2.24 us
  transfers between devices with their start and end apart: 3, of which 3 were waited for; matrix products, arithmetic and copies ran while one was open for 0% of the time, Pallas kernels for 0%

commit v1 on v0

--- a/solution.py
+++ b/solution.py
@@ -44,17 +44,25 @@
         jnp.bfloat16
     )
     answers = expert_rows(
-        lax.all_gather(
+        jnp.concatenate(
             lax.all_to_all(
-                outgoing.reshape(expert_count, capacity, hidden_state.shape[1]),
-                "ep",
-                split_axis=0,
-                concat_axis=0,
-                tiled=True,
+                jnp.stack(
+                    [
+                        lax.all_to_all(
+                            outgoing.reshape(expert_count, capacity, hidden_state.shape[1]),
+                            "ep",
+                            split_axis=0,
+                            concat_axis=0,
+                            tiled=True,
+                        )
+                    ]
+                    * lax.axis_size("tp")
+                ),
+                "tp",
+                0,
+                0,
             ),
-            "tp",
             axis=2,
-            tiled=True,
         ),
         gate_matrix,
         up_matrix,

time: 88.5 us -> 83.1 us (0.939)
  waiting for transfers between devices: 32.7 us -> 22.4 us
  blocking collectives: 24.2 us -> 28.6 us
  local copies, waits for them, and re-layouts: 1.65 us -> 3.23 us
  matrix products: 7.91 us -> 6.62 us
    all_gather x1 -> x0, waiting for transfers between devices: 8.17 us -> none  [shards(): lax.all_gather(lax.all_to_all(outgoing.reshape(expert_count, capacity, hi...]
    all_to_all x0 -> x1, blocking collectives: none -> 4.58 us  [shards(): lax.all_to_all(jnp.stack([lax.all_to_all(outgoing.reshape(expert_count, c...]
    reduce_scatter x1, waiting for transfers between devices: 9.7 us -> 7.57 us  [expert_rows(): lax.psum_scatter(partial_value.reshape(sources, item_count, feature_count...]
    dot_general x1, matrix products: 2.62 us -> 1.27 us  [expert_rows(): jnp.dot(token_rows, gate_matrix[0], preferred_element_type=jnp.float32)]
    reshape x0 -> x1, local copies, waits for them, and re-layouts: none -> 1.08 us  [shards(): jnp.concatenate(lax.all_to_all(jnp.stack([lax.all_to_all(outgoing.reshape...]
  transfers between devices with their start and end apart: 3 -> 2, of which waited for: 3 -> 2; matrix products, arithmetic and copies ran while one was open for 0% -> 0% of each run, Pallas kernels for 0% -> 0%
where the time goes in v1:
time: 83.1 us; the launch traced here: 82.7 us
  blocking collectives  28.6 us (34%)
  waiting for transfers between devices  22.4 us (27%)
  between operations  13.5 us (16%)
  matrix products  6.62 us (8%)
  starting transfers between devices  5.79 us (7%)
  local copies, waits for them, and re-layouts  3.23 us (4%)
  other arithmetic  2.5 us (3%)
    all_to_all x1, blocking collectives, shards(): lax.all_to_all(outgoing.reshape(expert_count, capacity, hidden_state.shap...  21.6 us
    all_to_all x1, waiting for transfers between devices, shards(): lax.all_to_all(answers, 'ep', split_axis=0, concat_axis=0, tiled=True)  14.8 us
    reduce_scatter x1, waiting for transfers between devices, expert_rows(): lax.psum_scatter(partial_value.reshape(sources, item_count, feature_count...  7.57 us
    all_to_all x1, starting transfers between devices, shards(): lax.all_to_all(answers, 'ep', split_axis=0, concat_axis=0, tiled=True)  5.78 us
    all_to_all x1, blocking collectives, shards(): lax.all_to_all(jnp.stack([lax.all_to_all(outgoing.reshape(expert_count, c...  4.58 us
    psum x1, blocking collectives, shards(): total_squares = lax.psum(local_squares, 'tp')  2.47 us
    dot_general x1, matrix products, expert_rows(): jnp.dot(activated, down_matrix[0], preferred_element_type=jnp.float32)  2.25 us
  transfers between devices with their start and end apart: 2, of which 2 were waited for; matrix products, arithmetic and copies ran while one was open for 0% of the time, Pallas kernels for 0%

profile of v1, /device:TPU:0, one launch (start us, length us, event | category | flops | bytes accessed | tf_op | source)
XLA Modules:
  0.0 82.7 jit_solution(12229881236951380764)
XLA Ops:
  6.5 0.0 copy-start
  6.5 0.0 reduce-scatter.2.cloned.1.call-start
  6.5 0.9 %copy.24 = s32[64,4]{1,0:T(8,128)S(1)} copy(s32[64,4]{0,1:T(4,128)} %param.8) | data formatting | bytes 2048 | tf_op args[1]
  7.5 0.1 eq.40
  7.6 0.6 reduce-window.6
  8.2 0.2 slice_reduce_fusion
  8.4 0.1 fusion.13
  8.5 0.1 reshape.139
  8.6 0.1 copy.25
  8.7 0.7 multiply_add_fusion
  9.4 0.1 fusion.11
  9.5 1.2 %convolution_convert_fusion = bf16[512,512]{1,0:T(8,128)(2,1)S(1)} fusion(pred[64,512]{1,0:T(8,128)(4,1)S(1)} %fusion.11, bf16[64,512]{1,0:T(8,128)(2,1)} %param.7), kind=kOutput, calls=%fused_computation.8 | convolution fusion | flops 33816576 | bytes 622592 | tf_op jit(solution)/shard_map/dot_general | solution.py:43
  10.7 21.6 %all_to_all.15 = bf16[8,64,512]{2,1,0:T(8,128)(2,1)S(1)} all-to-all(bf16[8,64,512]{2,1,0:T(8,128)(2,1)S(1)} %bitcast.48), channel_id=1, replica_groups=mesh['grp'=2,'ep'=8,'tp'=2] {'ep'}, dimensions={0} | all-to-all | bytes 1048576 | tf_op jit(solution)/shard_map/all_to_all | solution.py:51
  32.3 0.1 pad_maximum_fusion
  32.4 4.6 %all_to_all.16 = bf16[2,8,64,512]{3,2,1,0:T(8,128)(2,1)S(1)} all-to-all(bf16[2,8,64,512]{3,2,1,0:T(8,128)(2,1)S(1)} %pad_maximum_fusion), channel_id=1, replica_groups=mesh['grp'=2,'ep'=8,'tp'=2] {'tp'}, dimensions={0} | all-to-all | bytes 2097152 | tf_op jit(solution)/shard_map/all_to_all | solution.py:48
  37.0 1.1 %copy.26 = bf16[8,64,2,512]{3,2,1,0:T(2,128)(2,1)S(1)} copy(bf16[8,64,2,512]{3,1,0,2:T(8,128)(2,1)S(1)} %bitcast.44) | data formatting | bytes 2097152 | tf_op jit(solution)/shard_map/reshape | solution.py:47
  38.1 0.2 copy.27
  38.3 0.0 copy-done
  38.4 0.0 copy-start.3
  38.4 1.3 %fusion.4 = f32[512,1024]{1,0:T(8,128)S(1)} fusion(bf16[512,1024]{1,0:T(8,128)(2,1)S(1)} %bitcast.49, bf16[1,1024,1024]{2,1,0:T(8,128)(2,1)S(1)} %copy-done), kind=kOutput, calls=%fused_computation.4 | convolution fusion | flops 1073741824 | bytes 5242880 | tf_op jit(solution)/shard_map/dot_general | solution.py:19
  39.6 0.3 copy-done.3
  39.9 0.0 copy-start.4
  39.9 1.4 %multiply_convert_fusion = bf16[512,1024]{1,0:T(8,128)(2,1)S(1)} fusion(f32[512,1024]{1,0:T(8,128)S(1)} %fusion.4, bf16[512,1024]{1,0:T(8,128)(2,1)S(1)} %bitcast.50, bf16[1,1024,1024]{2,1,0:T(8,128)(2,1)S(1)} %copy-done.3), kind=kOutput, calls=%fused_computation.6 | convolution fusion | flops 1076887552 | bytes 6291456 | tf_op jit(solution)/shard_map/dot_general | solution.py:20
  41.4 0.2 copy-done.4
  41.5 2.3 %fusion.8 = bf16[8,64,1024]{2,1,0:T(8,128)(2,1)} fusion(bf16[8,64,1024]{2,1,0:T(8,128)(2,1)S(1)} %bitcast.52, bf16[1,1024,1024]{2,1,0:T(8,128)(2,1)S(1)} %copy-done.4), kind=kOutput, calls=%fused_computation.7 | convolution fusion | flops 1074266112 | bytes 4194304 | tf_op jit(solution)/shard_map/dot_general | solution.py:22
  43.8 0.0 copy-start.1
  43.8 0.0 copy-start.2
  43.8 0.0 reduce-scatter.2.cloned.1.call-update
  43.8 7.6 %reduce-scatter.2.cloned.1.call-done = bf16[8,64,512]{2,1,0:T(8,128)(2,1)} async-done(((bf16[8,64,1024]{2,1,0:T(8,128)(2,1)}), bf16[8,64,512]{2,1,0:T(8,128)(2,1)}) %reduce-scatter.2.cloned.1.call-update) | async-done | bytes 524304 | tf_op jit(solution)/shard_map/reduce_scatter | solution.py:23
  51.4 5.8 %all-to-all-start.2 = ((bf16[8,64,512]{2,1,0:T(8,128)(2,1)}), bf16[8,64,512]{2,1,0:T(8,128)(2,1)S(1)}, u32[]{:S(2)}, u32[]{:S(2)}) async-start(bf16[8,64,512]{2,1,0:T(8,128)(2,1)} %reduce-scatter.2.cloned.1.call-done), calls=%async_computation.3 | async-start | bytes 1048576 | tf_op jit(solution)/shard_map/all_to_all | solution.py:71
  57.2 0.0 copy-done.1
  57.2 0.1 select_reduce_fusion
  57.3 14.8 %all-to-all-done.2 = bf16[8,64,512]{2,1,0:T(8,128)(2,1)S(1)} async-done(((bf16[8,64,512]{2,1,0:T(8,128)(2,1)}), bf16[8,64,512]{2,1,0:T(8,128)(2,1)S(1)}, u32[]{:S(2)}, u32[]{:S(2)}) %all-to-all-start.2) | async-done | bytes 524320 | tf_op jit(solution)/shard_map/all_to_all | solution.py:71
  72.1 0.5 multiply_reduce_fusion
  72.6 2.5 %psum.7 = f32[64]{0:T(128)S(1)} all-reduce(f32[64]{0:T(128)S(1)} %get-tuple-element.5), channel_id=1, replica_groups=mesh['grp'=2,'ep'=8,'tp'=2] {'tp'}, use_global_device_ids=true, to_apply=%region_7.8 | all-reduce | flops 64 | bytes 512 | tf_op jit(solution)/shard_map/psum | solution.py:78
  75.1 0.0 copy-done.2
  75.1 0.7 multiply_convert_fusion.1
  (4 shorter events, 0.1 us)
Async XLA Ops:
  6.5 31.8 %copy-start = (bf16[1,1024,1024]{2,1,0:T(8,128)(2,1)S(1)}, bf16[1,1024,1024]{2,1,0:T(8,128)(2,1)}, u32[]{:S(2)}) copy-start(bf16[1,1024,1024]{2,1,0:T(8,128)(2,1)} %param.10) | copy-start | bytes 6291460
  6.5 44.9 %reduce-scatter.2.cloned.1.call-start = ((), (), s32[]{:S(2)}) async-start(), calls=%async_computation.4 | async-start | bytes 1572864 | tf_op jit(solution)/shard_map/reduce_scatter | solution.py:23
  38.4 1.6 %copy-start.3 = (bf16[1,1024,1024]{2,1,0:T(8,128)(2,1)S(1)}, bf16[1,1024,1024]{2,1,0:T(8,128)(2,1)}, u32[]{:S(2)}) copy-start(bf16[1,1024,1024]{2,1,0:T(8,128)(2,1)} %param.11) | copy-start | bytes 6291460
  39.9 1.6 %copy-start.4 = (bf16[1,1024,1024]{2,1,0:T(8,128)(2,1)S(1)}, bf16[1,1024,1024]{2,1,0:T(8,128)(2,1)}, u32[]{:S(2)}) copy-start(bf16[1,1024,1024]{2,1,0:T(8,128)(2,1)} %param.12) | copy-start | bytes 6291460
  43.8 13.4 %copy-start.1 = (f32[64,4]{0,1:T(4,128)S(1)}, f32[64,4]{0,1:T(4,128)}, u32[]{:S(2)}) copy-start(f32[64,4]{0,1:T(4,128)} %param.9) | copy-start | bytes 3076
  43.8 31.3 %copy-start.2 = (f32[512]{0:T(512)S(1)}, f32[512]{0:T(512)}, u32[]{:S(2)}) copy-start(f32[512]{0:T(512)} %param.13) | copy-start | bytes 6148
  51.4 20.7 %all-to-all-start.2 = ((bf16[8,64,512]{2,1,0:T(8,128)(2,1)}), bf16[8,64,512]{2,1,0:T(8,128)(2,1)S(1)}, u32[]{:S(2)}, u32[]{:S(2)}) async-start(bf16[8,64,512]{2,1,0:T(8,128)(2,1)} %reduce-scatter.2.cloned.1.call-done), calls=%async_computation.3 | async-start | bytes 1048576 | tf_op jit(solution)/shard_map/all_to_all | solution.py:71
Sparse Core Ops, SparseCore 0:
  43.9 7.4 reduce-scatter.1
